TPU v7x, 32 devices: a whole 2x2x4 slice. The times are simulated.
32 devices in a mesh: ep: 4 (over y, x), tp: 8 (over z, core).
Axes of the slice: x: 2, y: 2, z: 4, core: 2. Of those that a mesh axis runs over, the one named last changes fastest.
Arguments:
- tokens: bfloat16 [1024, 2048], P('ep', 'tp'), may hold values from -600 to 600
- pre_gain: float32 [2048], P('tp'), may hold values from 0.1 to 1.9
- expert_gate: bfloat16 [4, 2048, 8192], P('ep', None, 'tp'), may hold values from -0.125 to 0.125
- expert_up: bfloat16 [4, 2048, 8192], P('ep', None, 'tp'), may hold values from -0.125 to 0.125
- expert_down: bfloat16 [4, 8192, 2048], P('ep', 'tp'), may hold values from -8 to 8
- routes: int32 [1024, 2], P('ep'), may hold values from 0 to 3, all different within a row; in each aligned block of 256 rows (0 to 255, 256 to 511, ...) at most 192 rows name the same one
- route_weights: float32 [1024, 2], P('ep'), may hold values from 0.1 to 1
- post_gain: float32 [2048], P('tp'), may hold values from 0.1 to 1.9
Outputs:
- layer_out: bfloat16 [1024, 2048], P('ep', 'tp')
Inputs may be any that keep to these rules, and one draw needn't show every extreme that they name: `routes`: each token names 2 different experts. Among the 256 tokens of one index of ep no expert is named more than 192 times, a bound that some expert reaches in some of these blocks.
All inputs are finite; a program needn't handle non-finite values.
Results may differ from a plain program's by a relative error of at most 0.024.
Values may be sent and summed in bfloat16 or wider, within the bound.
A program may use at most 64 MiB of HBM per device.

v0:
```python
import jax
import jax.numpy as jnp
from jax import lax
from jax.sharding import PartitionSpec as P

EPSILON = 1e-06


def local(tokens, pre_gain, expert_gate, expert_up, expert_down, routes, route_weights, post_gain):
    local_experts = expert_gate.shape[0]
    groups = lax.axis_size("ep")
    experts_all = local_experts * groups
    tok_rows, part_width = tokens.shape
    full_width = part_width * lax.axis_size("tp")
    capacity = 3 * tok_rows // experts_all
    values = tokens.astype(jnp.float32)
    input_sq = lax.psum(jnp.sum(values * values, axis=-1), "tp")
    normed = (
        values * lax.rsqrt(input_sq / full_width + EPSILON)[:, None] * pre_gain[None, :]
    ).astype(jnp.bfloat16)
    onehot = (routes[:, :, None] == jnp.arange(experts_all, dtype=jnp.int32)).astype(jnp.int32)
    onehot = onehot.reshape(tok_rows * 2, experts_all)
    earlier = jnp.cumsum(onehot, axis=0) - onehot
    slots = jnp.sum(earlier * onehot, axis=-1).reshape(tok_rows, 2)
    positions = routes * capacity + slots
    places = jnp.arange(experts_all * capacity, dtype=jnp.int32)
    first_pick = (places[:, None] == positions[None, :, 0]).astype(jnp.bfloat16)
    second_pick = (places[:, None] == positions[None, :, 1]).astype(jnp.bfloat16)
    dispatch = first_pick + second_pick
    outgoing = jnp.dot(dispatch, normed, preferred_element_type=jnp.float32).astype(jnp.bfloat16)
    arrived = lax.all_to_all(outgoing, "ep", split_axis=0, concat_axis=0, tiled=True)
    fragment = lax.all_gather(arrived, "tp", axis=1, tiled=True)
    count = fragment.shape[1]
    grouped = fragment.reshape(groups, local_experts, capacity, count)
    gate_pre = jnp.einsum(
        "secw,ewf->secf", grouped, expert_gate, preferred_element_type=jnp.float32
    )
    up_pre = jnp.einsum("secw,ewf->secf", grouped, expert_up, preferred_element_type=jnp.float32)
    hidden = (jax.nn.silu(gate_pre) * up_pre).astype(jnp.bfloat16)
    product = jnp.einsum("secf,efd->dsec", hidden, expert_down, preferred_element_type=jnp.float32)
    summed = lax.psum_scatter(
        product.reshape(lax.axis_size("tp") * part_width, groups * local_experts * capacity).astype(
            jnp.bfloat16
        ),
        "tp",
        scatter_dimension=0,
        tiled=True,
    )
    returned = lax.all_to_all(summed, "ep", split_axis=1, concat_axis=1, tiled=True)
    contract = (((0,), (1,)), ((), ()))
    first_out = lax.dot_general(first_pick, returned, contract, preferred_element_type=jnp.float32)
    second_out = lax.dot_general(
        second_pick, returned, contract, preferred_element_type=jnp.float32
    )
    combined = route_weights[:, 0:1] * first_out + route_weights[:, 1:2] * second_out
    output_sq = lax.psum(jnp.sum(combined * combined, axis=-1), "tp")
    scaled = combined * lax.rsqrt(output_sq / full_width + EPSILON)[:, None] * post_gain[None, :]
    return scaled.astype(jnp.bfloat16)


def solution(mesh):
    placed = (
        P("ep", "tp"),
        P("tp"),
        P("ep", None, "tp"),
        P("ep", None, "tp"),
        P("ep", "tp", None),
        P("ep", None),
        P("ep", None),
        P("tp"),
    )
    return jax.shard_map(
        local, mesh=mesh, in_specs=placed, out_specs=P("ep", "tp"), check_vma=False
    )
```

profile of v0, /device:TPU:0, one launch (start us, length us, event | category | flops | bytes accessed | tf_op | source)
XLA Modules:
  0.0 164.0 jit_solution(8557718616161930768)
XLA Ops:
  6.5 0.0 all-gather.2.cloned.1.call-start
  6.5 0.8 copy.20
  7.4 0.1 eq.61
  7.5 0.1 eq.57
  7.7 1.2 reduce-window.6
  8.9 0.2 slice_reduce_fusion
  9.1 0.2 reduce-window.9
  9.3 0.1 add_bitcast_fusion
  9.4 0.1 reshape.55
  9.5 0.1 copy.22
  9.6 0.7 multiply_add_fusion
  10.3 1.0 fusion.28
  11.3 18.1 %psum.14 = f32[256]{0:T(256)S(1)} all-reduce(f32[256]{0:T(256)S(1)} %fusion.28), channel_id=1, replica_groups=mesh['ep'=4,'tp'=8] {'tp'}, use_global_device_ids=true, to_apply=%region_4.5 | all-reduce | flops 256 | bytes 2048 | tf_op jit(solution)/shard_map/psum | solution.py:17
  29.4 1.3 convolution_convert_fusion
  30.7 10.1 %all_to_all.24 = bf16[4,192,256]{2,1,0:T(8,128)(2,1)} all-to-all(bf16[4,192,256]{2,1,0:T(8,128)(2,1)S(1)} %bitcast.82), channel_id=1, replica_groups=mesh['ep'=4,'tp'=8] {'ep'}, dimensions={0} | all-to-all | bytes 786432 | tf_op jit(solution)/shard_map/all_to_all | solution.py:31
  40.8 0.0 all-gather.2.cloned.1.call-update
  40.8 0.0 reduce-scatter.2.cloned.1.call-start
  40.8 35.9 %all-gather.2.cloned.1.call-done = bf16[768,2048]{1,0:T(8,128)(2,1)} async-done(((bf16[768,256]{1,0:T(8,128)(2,1)}), bf16[768,2048]{1,0:T(8,128)(2,1)}) %all-gather.2.cloned.1.call-update) | async-done | bytes 3145744 | tf_op jit(solution)/shard_map/all_gather | solution.py:32
  76.8 0.0 copy-start.2
  76.8 0.0 copy-start.4
  76.8 6.3 %fusion.2 = f32[4,192,1024]{2,1,0:T(8,128)S(1)} fusion(bf16[4,192,2048]{2,1,0:T(8,128)(2,1)} %bitcast.90, bf16[1,2048,1024]{2,1,0:T(8,128)(2,1)} %param.11), kind=kOutput, calls=%fused_computation.2 | convolution fusion | flops 3221225472 | bytes 10485760 | tf_op jit(solution)/shard_map/secw,ewf->secf/dot_general | solution.py:38
  83.1 0.0 copy-done.2
  83.1 0.0 copy-done.4
  83.1 0.0 copy-start.3
  83.1 3.8 %fusion.9 = bf16[4,1,192,1024]{3,2,0,1:T(8,128)(2,1)S(1)} fusion(f32[4,192,1024]{2,1,0:T(8,128)S(1)} %fusion.2, bf16[4,192,2048]{2,1,0:T(8,128)(2,1)S(1)} %bitcast.91, bf16[1,2048,1024]{2,1,0:T(8,128)(2,1)S(1)} %copy-done.2), kind=kOutput, calls=%fused_computation.8 | convolution fusion | flops 3225944064 | bytes 12058624 | tf_op jit(solution)/shard_map/secw,ewf->secf/dot_general | solution.py:35
  87.0 0.0 copy-done.3
  87.0 4.8 %fusion.13 = bf16[2048,768]{0,1:T(8,128)(2,1)} fusion(bf16[768,1024]{1,0:T(8,128)(2,1)S(1)} %bitcast.92, bf16[1,1024,2048]{2,1,0:T(8,128)(2,1)S(1)} %copy-done.3), kind=kOutput, calls=%fused_computation.14 | convolution fusion | flops 3222798336 | bytes 8912896 | tf_op jit(solution)/shard_map/secf,efd->dsec/dot_general | solution.py:40
  91.8 0.0 copy-start
  91.8 0.0 copy-start.1
  91.8 0.0 reduce-scatter.2.cloned.1.call-update
  91.8 38.8 %reduce-scatter.2.cloned.1.call-done = bf16[256,768]{0,1:T(8,128)(2,1)} async-done(((bf16[2048,768]{0,1:T(8,128)(2,1)}), bf16[256,768]{0,1:T(8,128)(2,1)}) %reduce-scatter.2.cloned.1.call-update) | async-done | bytes 393232 | tf_op jit(solution)/shard_map/reduce_scatter | solution.py:41
  130.6 3.6 %all-to-all-start.1 = ((bf16[256,4,192]{0,2,1:T(8,128)(2,1)}), bf16[256,4,192]{0,2,1:T(8,128)(2,1)S(1)}, u32[]{:S(2)}, u32[]{:S(2)}) async-start(bf16[256,4,192]{0,2,1:T(8,128)(2,1)} %bitcast.81), calls=%async_computation.2 | async-start | bytes 786432 | tf_op jit(solution)/shard_map/all_to_all | solution.py:49
  134.2 0.0 copy-done
  134.2 5.9 %all-to-all-done.1 = bf16[256,4,192]{0,2,1:T(8,128)(2,1)S(1)} async-done(((bf16[256,4,192]{0,2,1:T(8,128)(2,1)}), bf16[256,4,192]{0,2,1:T(8,128)(2,1)S(1)}, u32[]{:S(2)}, u32[]{:S(2)}) %all-to-all-start.1) | async-done | bytes 393248 | tf_op jit(solution)/shard_map/all_to_all | solution.py:49
  140.1 0.4 convolution_multiply_fusion.1
  140.5 0.4 multiply_reduce_fusion
  140.9 15.4 %psum.15 = f32[256]{0:T(256)S(1)} all-reduce(f32[256]{0:T(256)S(1)} %get-tuple-element.9), channel_id=1, replica_groups=mesh['ep'=4,'tp'=8] {'tp'}, use_global_device_ids=true, to_apply=%region_7.8 | all-reduce | flops 256 | bytes 2048 | tf_op jit(solution)/shard_map/psum | solution.py:56
  156.3 0.0 copy-done.1
  156.3 0.1 multiply_convert_fusion
  156.4 0.8 copy.23
  (6 shorter events, 0.1 us)
Async XLA Ops:
  6.5 70.3 %all-gather.2.cloned.1.call-start = ((), (), s32[]{:S(2)}) async-start(), calls=%async_computation.3 | async-start | bytes 3538944 | tf_op jit(solution)/shard_map/all_gather | solution.py:32
  40.8 89.8 %reduce-scatter.2.cloned.1.call-start = ((), (), s32[]{:S(2)}) async-start(), calls=%async_computation.4 | async-start | bytes 3538944 | tf_op jit(solution)/shard_map/reduce_scatter | solution.py:41
  76.8 6.3 %copy-start.2 = (bf16[1,2048,1024]{2,1,0:T(8,128)(2,1)S(1)}, bf16[1,2048,1024]{2,1,0:T(8,128)(2,1)}, u32[]{:S(2)}) copy-start(bf16[1,2048,1024]{2,1,0:T(8,128)(2,1)} %param.10) | copy-start | bytes 12582916
  76.8 6.3 %copy-start.4 = (bf16[768,2048]{1,0:T(8,128)(2,1)S(1)}, bf16[768,2048]{1,0:T(8,128)(2,1)}, u32[]{:S(2)}) copy-start(bf16[768,2048]{1,0:T(8,128)(2,1)} %all-gather.2.cloned.1.call-done) | copy-start | bytes 9437188
  83.1 3.9 %copy-start.3 = (bf16[1,1024,2048]{2,1,0:T(8,128)(2,1)S(1)}, bf16[1,1024,2048]{2,1,0:T(8,128)(2,1)}, u32[]{:S(2)}) copy-start(bf16[1,1024,2048]{2,1,0:T(8,128)(2,1)} %param.12) | copy-start | bytes 12582916
  91.8 42.4 %copy-start = (f32[256,2]{0,1:T(2,128)S(1)}, f32[256,2]{0,1:T(2,128)}, u32[]{:S(2)}) copy-start(f32[256,2]{0,1:T(2,128)} %param.14) | copy-start | bytes 6148
  91.8 64.5 %copy-start.1 = (f32[256]{0:T(256)S(1)}, f32[256]{0:T(256)}, u32[]{:S(2)}) copy-start(f32[256]{0:T(256)} %param.15) | copy-start | bytes 3076
  130.6 9.5 %all-to-all-start.1 = ((bf16[256,4,192]{0,2,1:T(8,128)(2,1)}), bf16[256,4,192]{0,2,1:T(8,128)(2,1)S(1)}, u32[]{:S(2)}, u32[]{:S(2)}) async-start(bf16[256,4,192]{0,2,1:T(8,128)(2,1)} %bitcast.81), calls=%async_computation.2 | async-start | bytes 786432 | tf_op jit(solution)/shard_map/all_to_all | solution.py:49
Sparse Core Ops, SparseCore 0:
  40.9 35.8 all-gather.1
  91.9 38.5 reduce-scatter.1
where the time goes:
time: 164 us
  waiting for transfers between devices  80.6 us (49%)
  blocking collectives  43.6 us (27%)
  matrix products  17 us (10%)
  between operations  13.5 us (8%)
  starting transfers between devices  3.69 us (2%)
  other arithmetic  3.35 us (2%)
  local copies, waits for them, and re-layouts  2.31 us (1%)
    reduce_scatter x1, waiting for transfers between devices, local(): lax.psum_scatter(product.reshape(lax.axis_size('tp') * part_width, groups...  38.8 us
    all_gather x1, waiting for transfers between devices, local(): fragment = lax.all_gather(arrived, 'tp', axis=1, tiled=True)  35.9 us
    psum x1, blocking collectives, local(): input_sq = lax.psum(jnp.sum(values * values, axis=-1), 'tp')  18.1 us
    psum x1, blocking collectives, local(): output_sq = lax.psum(jnp.sum(combined * combined, axis=-1), 'tp')  15.4 us
    all_to_all x1, blocking collectives, local(): lax.all_to_all(outgoing, 'ep', split_axis=0, concat_axis=0, tiled=True)  10.1 us
    dot_general x1, matrix products, local(): jnp.einsum('secw,ewf->secf', grouped, expert_up, preferred_element_type=j...  6.28 us
    all_to_all x1, waiting for transfers between devices, local(): lax.all_to_all(summed, 'ep', split_axis=1, concat_axis=1, tiled=True)  5.87 us
    dot_general x1, matrix products, local(): jnp.einsum('secf,efd->dsec', hidden, expert_down, preferred_element_type=...  4.83 us
  transfers between devices with their start and end apart: 3, of which 3 were waited for; matrix products, arithmetic and copies ran while one was open for 0% of the time, Pallas kernels for 0%

commit v1 on v0

--- a/solution.py
+++ b/solution.py
@@ -53,7 +53,9 @@
         second_pick, returned, contract, preferred_element_type=jnp.float32
     )
     combined = route_weights[:, 0:1] * first_out + route_weights[:, 1:2] * second_out
-    output_sq = lax.psum(jnp.sum(combined * combined, axis=-1), "tp")
+    block = jnp.sum(combined * combined, axis=-1)
+    parts = lax.all_gather(block, "tp")
+    output_sq = jnp.sum(parts, axis=0)
     scaled = combined * lax.rsqrt(output_sq / full_width + EPSILON)[:, None] * post_gain[None, :]
     return scaled.astype(jnp.bfloat16)
 

time: 164 us -> 159 us (0.970)
  blocking collectives: 43.6 us -> 38.4 us
    psum x1 -> x0, blocking collectives: 15.4 us -> none  [local(): output_sq = lax.psum(jnp.sum(combined * combined, axis=-1), 'tp')]
    all_gather x0 -> x1, blocking collectives: none -> 10.3 us  [local(): parts = lax.all_gather(block, 'tp')]
where the time goes in v1:
time: 159 us
  waiting for transfers between devices  80.6 us (51%)
  blocking collectives  38.4 us (24%)
  matrix products  17 us (11%)
  between operations  13.5 us (8%)
  starting transfers between devices  3.69 us (2%)
  other arithmetic  3.38 us (2%)
  local copies, waits for them, and re-layouts  2.31 us (1%)
    reduce_scatter x1, waiting for transfers between devices, local(): lax.psum_scatter(product.reshape(lax.axis_size('tp') * part_width, groups...  38.8 us
    all_gather x1, waiting for transfers between devices, local(): fragment = lax.all_gather(arrived, 'tp', axis=1, tiled=True)  35.9 us
    psum x1, blocking collectives, local(): input_sq = lax.psum(jnp.sum(values * values, axis=-1), 'tp')  18.1 us
    all_gather x1, blocking collectives, local(): parts = lax.all_gather(block, 'tp')  10.3 us
    all_to_all x1, blocking collectives, local(): lax.all_to_all(outgoing, 'ep', split_axis=0, concat_axis=0, tiled=True)  10.1 us
    dot_general x1, matrix products, local(): jnp.einsum('secw,ewf->secf', grouped, expert_up, preferred_element_type=j...  6.28 us
    all_to_all x1, waiting for transfers between devices, local(): lax.all_to_all(summed, 'ep', split_axis=1, concat_axis=1, tiled=True)  5.87 us
    dot_general x1, matrix products, local(): jnp.einsum('secf,efd->dsec', hidden, expert_down, preferred_element_type=...  4.83 us
  transfers between devices with their start and end apart: 3, of which 3 were waited for; matrix products, arithmetic and copies ran while one was open for 0% of the time, Pallas kernels for 0%

profile of v1, /device:TPU:0, one launch (start us, length us, event | category | flops | bytes accessed | tf_op | source)
XLA Modules:
  0.0 158.9 jit_solution(1153129783960446045)
XLA Ops:
  6.5 0.0 all-gather.4.cloned.1.call-start
  6.5 0.8 copy.25
  7.4 0.1 eq.61
  7.5 0.1 eq.57
  7.7 1.2 reduce-window.6
  8.9 0.2 slice_reduce_fusion
  9.1 0.2 reduce-window.9
  9.3 0.1 add_bitcast_fusion
  9.4 0.1 reshape.59
  9.5 0.1 copy.27
  9.6 0.7 multiply_add_fusion
  10.3 1.0 fusion.28
  11.3 18.1 %psum.7 = f32[256]{0:T(256)S(1)} all-reduce(f32[256]{0:T(256)S(1)} %fusion.28), channel_id=1, replica_groups=mesh['ep'=4,'tp'=8] {'tp'}, use_global_device_ids=true, to_apply=%region_4.5 | all-reduce | flops 256 | bytes 2048 | tf_op jit(solution)/shard_map/psum | solution.py:17
  29.4 1.3 convolution_convert_fusion
  30.7 10.1 %all_to_all.24 = bf16[4,192,256]{2,1,0:T(8,128)(2,1)} all-to-all(bf16[4,192,256]{2,1,0:T(8,128)(2,1)S(1)} %bitcast.83), channel_id=1, replica_groups=mesh['ep'=4,'tp'=8] {'ep'}, dimensions={0} | all-to-all | bytes 786432 | tf_op jit(solution)/shard_map/all_to_all | solution.py:31
  40.8 0.0 all-gather.4.cloned.1.call-update
  40.8 0.0 reduce-scatter.2.cloned.1.call-start
  40.8 35.9 %all-gather.4.cloned.1.call-done = bf16[768,2048]{1,0:T(8,128)(2,1)} async-done(((bf16[768,256]{1,0:T(8,128)(2,1)}), bf16[768,2048]{1,0:T(8,128)(2,1)}) %all-gather.4.cloned.1.call-update) | async-done | bytes 3145744 | tf_op jit(solution)/shard_map/all_gather | solution.py:32
  76.8 0.0 copy-start.2
  76.8 0.0 copy-start.4
  76.8 6.3 %fusion.2 = f32[4,192,1024]{2,1,0:T(8,128)S(1)} fusion(bf16[4,192,2048]{2,1,0:T(8,128)(2,1)} %bitcast.92, bf16[1,2048,1024]{2,1,0:T(8,128)(2,1)} %param.11), kind=kOutput, calls=%fused_computation.2 | convolution fusion | flops 3221225472 | bytes 10485760 | tf_op jit(solution)/shard_map/secw,ewf->secf/dot_general | solution.py:38
  83.1 0.0 copy-done.2
  83.1 0.0 copy-done.4
  83.1 0.0 copy-start.3
  83.1 3.8 %fusion.9 = bf16[4,1,192,1024]{3,2,0,1:T(8,128)(2,1)S(1)} fusion(f32[4,192,1024]{2,1,0:T(8,128)S(1)} %fusion.2, bf16[4,192,2048]{2,1,0:T(8,128)(2,1)S(1)} %bitcast.93, bf16[1,2048,1024]{2,1,0:T(8,128)(2,1)S(1)} %copy-done.2), kind=kOutput, calls=%fused_computation.8 | convolution fusion | flops 3225944064 | bytes 12058624 | tf_op jit(solution)/shard_map/secw,ewf->secf/dot_general | solution.py:35
  87.0 0.0 copy-done.3
  87.0 4.8 %fusion.13 = bf16[2048,768]{0,1:T(8,128)(2,1)} fusion(bf16[768,1024]{1,0:T(8,128)(2,1)S(1)} %bitcast.94, bf16[1,1024,2048]{2,1,0:T(8,128)(2,1)S(1)} %copy-done.3), kind=kOutput, calls=%fused_computation.14 | convolution fusion | flops 3222798336 | bytes 8912896 | tf_op jit(solution)/shard_map/secf,efd->dsec/dot_general | solution.py:40
  91.8 0.0 copy-start
  91.8 0.0 copy-start.1
  91.8 0.0 reduce-scatter.2.cloned.1.call-update
  91.8 38.8 %reduce-scatter.2.cloned.1.call-done = bf16[256,768]{0,1:T(8,128)(2,1)} async-done(((bf16[2048,768]{0,1:T(8,128)(2,1)}), bf16[256,768]{0,1:T(8,128)(2,1)}) %reduce-scatter.2.cloned.1.call-update) | async-done | bytes 393232 | tf_op jit(solution)/shard_map/reduce_scatter | solution.py:41
  130.6 3.6 %all-to-all-start.1 = ((bf16[256,4,192]{0,2,1:T(8,128)(2,1)}), bf16[256,4,192]{0,2,1:T(8,128)(2,1)S(1)}, u32[]{:S(2)}, u32[]{:S(2)}) async-start(bf16[256,4,192]{0,2,1:T(8,128)(2,1)} %bitcast.82), calls=%async_computation.2 | async-start | bytes 786432 | tf_op jit(solution)/shard_map/all_to_all | solution.py:49
  134.2 0.0 copy-done
  134.2 5.9 %all-to-all-done.1 = bf16[256,4,192]{0,2,1:T(8,128)(2,1)S(1)} async-done(((bf16[256,4,192]{0,2,1:T(8,128)(2,1)}), bf16[256,4,192]{0,2,1:T(8,128)(2,1)S(1)}, u32[]{:S(2)}, u32[]{:S(2)}) %all-to-all-start.1) | async-done | bytes 393248 | tf_op jit(solution)/shard_map/all_to_all | solution.py:49
  140.1 0.4 convolution_multiply_fusion.1
  140.5 0.4 multiply_reduce_fusion
  140.9 10.3 %all-gather.1 = f32[8,1,256]{2,1,0:T(1,128)S(1)} all-gather(f32[1,1,256]{2,1,0:T(1,128)S(1)} %bitcast.85), channel_id=2, replica_groups=mesh['ep'=4,'tp'=8] {'tp'}, dimensions={0}, use_global_device_ids=true | all-gather | bytes 9216 | tf_op jit(solution)/shard_map/all_gather | solution.py:57
  151.2 0.0 copy-done.1
  151.2 0.1 multiply_convert_fusion
  151.3 0.8 copy.28
  (7 shorter events, 0.1 us)
Async XLA Ops:
  6.5 70.3 %all-gather.4.cloned.1.call-start = ((), (), s32[]{:S(2)}) async-start(), calls=%async_computation.3 | async-start | bytes 3538944 | tf_op jit(solution)/shard_map/all_gather | solution.py:32
  40.8 89.8 %reduce-scatter.2.cloned.1.call-start = ((), (), s32[]{:S(2)}) async-start(), calls=%async_computation.4 | async-start | bytes 3538944 | tf_op jit(solution)/shard_map/reduce_scatter | solution.py:41
  76.8 6.3 %copy-start.2 = (bf16[1,2048,1024]{2,1,0:T(8,128)(2,1)S(1)}, bf16[1,2048,1024]{2,1,0:T(8,128)(2,1)}, u32[]{:S(2)}) copy-start(bf16[1,2048,1024]{2,1,0:T(8,128)(2,1)} %param.10) | copy-start | bytes 12582916
  76.8 6.3 %copy-start.4 = (bf16[768,2048]{1,0:T(8,128)(2,1)S(1)}, bf16[768,2048]{1,0:T(8,128)(2,1)}, u32[]{:S(2)}) copy-start(bf16[768,2048]{1,0:T(8,128)(2,1)} %all-gather.4.cloned.1.call-done) | copy-start | bytes 9437188
  83.1 3.9 %copy-start.3 = (bf16[1,1024,2048]{2,1,0:T(8,128)(2,1)S(1)}, bf16[1,1024,2048]{2,1,0:T(8,128)(2,1)}, u32[]{:S(2)}) copy-start(bf16[1,1024,2048]{2,1,0:T(8,128)(2,1)} %param.12) | copy-start | bytes 12582916
  91.8 42.4 %copy-start = (f32[256,2]{0,1:T(2,128)S(1)}, f32[256,2]{0,1:T(2,128)}, u32[]{:S(2)}) copy-start(f32[256,2]{0,1:T(2,128)} %param.14) | copy-start | bytes 6148
  91.8 59.4 %copy-start.1 = (f32[256]{0:T(256)S(1)}, f32[256]{0:T(256)}, u32[]{:S(2)}) copy-start(f32[256]{0:T(256)} %param.15) | copy-start | bytes 3076
  130.6 9.5 %all-to-all-start.1 = ((bf16[256,4,192]{0,2,1:T(8,128)(2,1)}), bf16[256,4,192]{0,2,1:T(8,128)(2,1)S(1)}, u32[]{:S(2)}, u32[]{:S(2)}) async-start(bf16[256,4,192]{0,2,1:T(8,128)(2,1)} %bitcast.82), calls=%async_computation.2 | async-start | bytes 786432 | tf_op jit(solution)/shard_map/all_to_all | solution.py:49
Sparse Core Ops, SparseCore 0:
  40.9 35.8 all-gather.3
  91.9 38.5 reduce-scatter.1
